TPU v7x, 32 devices: a whole 2x2x4 slice. The times are simulated.
32 devices in a mesh: sp: 4 (over z), dp: 8 (over y, x, core).
Axes of the slice: x: 2, y: 2, z: 4, core: 2. Of those that a mesh axis runs over, the one named last changes fastest.
Arguments:
- probe_vectors: bfloat16 [4096, 1024], P(('dp', 'sp')), may hold values from -6 to 6
- address_vectors: bfloat16 [4096, 1024], P(('dp', 'sp')), may hold values from -6 to 6
- content_vectors: bfloat16 [4096, 2048], P(('dp', 'sp')), may hold values from -6 to 6
- adjoint_of_result: bfloat16 [4096, 2048], P(('dp', 'sp')), may hold values from -0.5 to 0.5
- compact_factor: bfloat16 [4096, 64], P(('dp', 'sp')), may hold values from -7.5 to 7.5
- latent_to_damping_map: bfloat16 [64, 1024], replicated, may hold values from -0.75 to 0.75
- damping_shift_term: float32 [1024], replicated
- surplus_damping: bfloat16 [4096, 16], P(('dp', 'sp')), may hold values from -0.7 to 0
Outputs:
- query_grad: bfloat16 [4096, 1024], P(('dp', 'sp'))
- key_grad: bfloat16 [4096, 1024], P(('dp', 'sp'))
- value_grad: bfloat16 [4096, 2048], P(('dp', 'sp'))
- latent_grad: bfloat16 [4096, 64], P(('dp', 'sp'))
- weight_grad: float32 [64, 1024], replicated
All inputs are finite; a program needn't handle non-finite values.
Results may differ from a plain program's by a relative error of at most 0.005.
Values may be sent and summed in bfloat16 or wider, within the bound.
No kernel may reach another device: no remote copies, remote signals or barrier semaphores. Data moves between devices by JAX's collectives and lax.ppermute only.
A program may use at most 64 MiB of HBM per device.

v0:
```python
import jax
import jax.numpy as jnp
from jax import lax
from jax.sharding import PartitionSpec as P

KEY_CHANNELS = 64
VALUE_DIM = 128
BLOCK = 64
gate_norm = 16.0
highest = lax.Precision.HIGHEST


def carry_states(block_total, increments):
    log_totals = block_total[:, :, 0, :]
    running = jnp.cumsum(log_totals, axis=1)
    before = running - log_totals
    blocks = log_totals.shape[1]
    order = jnp.arange(blocks, dtype=jnp.int32)
    earlier_mask = (order[None, :] < order[:, None])[None, :, :, None]
    exponent = before[:, :, None, :] - running[:, None, :, :]
    exponent = jnp.where(earlier_mask, exponent, jnp.zeros_like(exponent))
    weights = jnp.where(earlier_mask, jnp.exp(exponent), jnp.zeros_like(exponent))
    return jnp.einsum("hnmk,mhkv->nhkv", weights, increments, precision=highest)


def gla_forward(probe_vectors, address_vectors, content_vectors, logarithm_decay):
    head_count, seq_len, key_width = probe_vectors.shape
    value_width = content_vectors.shape[2]
    blocks = seq_len // BLOCK

    def blocked(tensor):
        return tensor.reshape(head_count, blocks, BLOCK, tensor.shape[2])

    cumulative = jnp.cumsum(blocked(logarithm_decay), axis=2)
    block_total = cumulative[:, :, BLOCK - 1 :, :]
    keys_block = blocked(address_vectors)
    query_decayed = blocked(probe_vectors) * key_width ** (-0.5) * jnp.exp(cumulative)
    key_inverse = keys_block * jnp.exp(-cumulative)
    key_to_end = keys_block * jnp.exp(block_total - cumulative)
    value_block = blocked(content_vectors)
    scores = jnp.einsum("hnik,hnjk->hnij", query_decayed, key_inverse, precision=highest)
    positions = jnp.arange(BLOCK, dtype=jnp.int32)
    causal = positions[:, None] >= positions[None, :]
    scores = jnp.where(causal, scores, jnp.zeros_like(scores))
    within_block = jnp.einsum("hnij,hnjv->hniv", scores, value_block, precision=highest)
    increments = jnp.einsum("hnjk,hnjv->nhkv", key_to_end, value_block, precision=highest)
    earlier = carry_states(block_total, increments)
    carried = jnp.einsum("hnik,nhkv->hniv", query_decayed, earlier, precision=highest)
    return (within_block + carried).reshape(head_count, seq_len, value_width)


def split_into_heads(tensor, width):
    return tensor.astype(jnp.float32).reshape(tensor.shape[0], -1, width).transpose(1, 0, 2)


def to_rows(tensor):
    return tensor.transpose(1, 0, 2).reshape(tensor.shape[1], tensor.shape[0] * tensor.shape[2])


def on_device(
    probe_vectors,
    address_vectors,
    content_vectors,
    adjoint_of_result,
    compact_factor,
    latent_to_damping_map,
    damping_shift_term,
    surplus_damping,
):
    query_per_head, key_per_head, value_per_head, upstream_heads, spike_heads = (
        lax.all_to_all(probe_vectors, "sp", split_axis=1, concat_axis=0, tiled=True),
        lax.all_to_all(address_vectors, "sp", split_axis=1, concat_axis=0, tiled=True),
        lax.all_to_all(content_vectors, "sp", split_axis=1, concat_axis=0, tiled=True),
        lax.all_to_all(adjoint_of_result, "sp", split_axis=1, concat_axis=0, tiled=True),
        lax.all_to_all(surplus_damping, "sp", split_axis=1, concat_axis=0, tiled=True),
    )
    local_width = query_per_head.shape[1]
    hidden_code_rows = lax.all_gather(compact_factor, "sp", axis=0, tiled=True)
    column_start = lax.axis_index("sp") * local_width
    weight_local = lax.dynamic_slice_in_dim(latent_to_damping_map, column_start, local_width, 1)
    bias_local = lax.dynamic_slice_in_dim(damping_shift_term, column_start, local_width, 0)
    gate_logit = (
        jnp.dot(hidden_code_rows, weight_local, preferred_element_type=jnp.float32) + bias_local
    )
    forget_rate_rows = jax.nn.log_sigmoid(gate_logit) / gate_norm
    logarithm_decay = (
        split_into_heads(forget_rate_rows, KEY_CHANNELS)
        + spike_heads.astype(jnp.float32).T[:, :, None]
    )
    _, pullback = jax.vjp(
        gla_forward,
        split_into_heads(query_per_head, KEY_CHANNELS),
        split_into_heads(key_per_head, KEY_CHANNELS),
        split_into_heads(value_per_head, VALUE_DIM),
        logarithm_decay,
    )
    grad_query, grad_key, grad_value, grad_decay = pullback(
        split_into_heads(upstream_heads, VALUE_DIM)
    )
    query_grad, key_grad, value_grad = (
        lax.all_to_all(
            to_rows(grad_query).astype(jnp.bfloat16), "sp", split_axis=0, concat_axis=1, tiled=True
        ),
        lax.all_to_all(
            to_rows(grad_key).astype(jnp.bfloat16), "sp", split_axis=0, concat_axis=1, tiled=True
        ),
        lax.all_to_all(
            to_rows(grad_value).astype(jnp.bfloat16), "sp", split_axis=0, concat_axis=1, tiled=True
        ),
    )
    decay_rows = to_rows(grad_decay)
    gate_grad = (decay_rows * jax.nn.sigmoid(-gate_logit) / gate_norm).astype(jnp.bfloat16)
    partial_latent = jnp.einsum(
        "sc,rc->sr", gate_grad, weight_local, preferred_element_type=jnp.float32
    )
    latent_grad = lax.psum_scatter(partial_latent, "sp", scatter_dimension=0, tiled=True).astype(
        jnp.bfloat16
    )
    local_weight = jnp.einsum(
        "sr,sc->rc", hidden_code_rows, gate_grad, preferred_element_type=jnp.float32
    )
    summed = lax.psum(local_weight, "dp")
    weight_grad = lax.all_gather(summed, "sp", axis=1, tiled=True)
    return (query_grad, key_grad, value_grad, latent_grad, weight_grad)


def solution(mesh):
    return jax.shard_map(
        on_device,
        mesh=mesh,
        in_specs=(
            P(("dp", "sp"), None),
            P(("dp", "sp"), None),
            P(("dp", "sp"), None),
            P(("dp", "sp"), None),
            P(("dp", "sp"), None),
            P(),
            P(),
            P(("dp", "sp"), None),
        ),
        out_specs=(
            P(("dp", "sp"), None),
            P(("dp", "sp"), None),
            P(("dp", "sp"), None),
            P(("dp", "sp"), None),
            P(),
        ),
        check_vma=False,
    )
```

profile of v0, /device:TPU:0, one launch (start us, length us, event | category | flops | bytes accessed | tf_op | source)
XLA Modules:
  0.0 277.0 jit_solution(3052615414394250195)
XLA Ops:
  8.0 6.5 %all-to-all-start.1 = ((bf16[128,4,4]{0,2,1:T(4,128)(2,1)}), bf16[128,4,4]{0,2,1:T(4,128)(2,1)S(1)}, u32[]{:S(2)}, u32[]{:S(2)}) async-start(bf16[128,4,4]{0,2,1:T(4,128)(2,1)} %bitcast.169), calls=%async_computation.1 | async-start | bytes 8192 | tf_op jit(solution)/shard_map/all_to_all | solution.py:75
  14.5 1.8 copy.214
  16.3 3.8 %all-to-all-done.1 = bf16[128,4,4]{0,2,1:T(4,128)(2,1)S(1)} async-done(((bf16[128,4,4]{0,2,1:T(4,128)(2,1)}), bf16[128,4,4]{0,2,1:T(4,128)(2,1)S(1)}, u32[]{:S(2)}, u32[]{:S(2)}) %all-to-all-start.1) | async-done | bytes 4128 | tf_op jit(solution)/shard_map/all_to_all | solution.py:75
  20.1 3.5 %all-to-all-start.5 = ((bf16[128,4,256]{0,2,1:T(8,128)(2,1)}), bf16[128,4,256]{0,2,1:T(8,128)(2,1)S(1)}, u32[]{:S(2)}, u32[]{:S(2)}) async-start(bf16[128,4,256]{0,2,1:T(8,128)(2,1)} %bitcast.24), calls=%async_computation.5 | async-start | bytes 524288 | tf_op jit(solution)/shard_map/all_to_all | solution.py:71
  24.5 7.0 %all-to-all-done.5 = bf16[128,4,256]{0,2,1:T(8,128)(2,1)S(1)} async-done(((bf16[128,4,256]{0,2,1:T(8,128)(2,1)}), bf16[128,4,256]{0,2,1:T(8,128)(2,1)S(1)}, u32[]{:S(2)}, u32[]{:S(2)}) %all-to-all-start.5) | async-done | bytes 262176 | tf_op jit(solution)/shard_map/all_to_all | solution.py:71
  31.5 3.4 %all-to-all-start = ((bf16[128,4,256]{0,2,1:T(8,128)(2,1)}), bf16[128,4,256]{0,2,1:T(8,128)(2,1)S(1)}, u32[]{:S(2)}, u32[]{:S(2)}) async-start(bf16[128,4,256]{0,2,1:T(8,128)(2,1)} %bitcast), calls=%async_computation | async-start | bytes 524288 | tf_op jit(solution)/shard_map/all_to_all | solution.py:72
  36.6 12.5 %all_gather.6 = bf16[512,64]{0,1:T(8,128)(2,1)S(1)} all-gather(bf16[128,64]{0,1:T(8,128)(2,1)S(1)} %copy-done.31), channel_id=1, replica_groups=mesh['sp'=4,'dp'=8] {'sp'}, dimensions={0}, use_global_device_ids=true | all-gather | bytes 81920 | tf_op jit(solution)/shard_map/all_gather | solution.py:78
  51.7 4.1 %all-to-all-start.3 = ((bf16[128,4,512]{2,0,1:T(8,128)(2,1)}), bf16[128,4,512]{2,0,1:T(8,128)(2,1)}, u32[]{:S(2)}, u32[]{:S(2)}) async-start(bf16[128,4,512]{2,0,1:T(8,128)(2,1)} %bitcast.143), calls=%async_computation.3 | async-start | bytes 1048576 | tf_op jit(solution)/shard_map/all_to_all | solution.py:74
  58.0 25.9 %fusion.46 = f32[4,8,64,64]{3,1,2,0:T(8,128)S(1)} fusion(f32[4,8,64,64]{3,1,2,0:T(8,128)S(1)} %copy.194), kind=kOutput, calls=%fused_computation.84 | output fusion | flops 8257536 | bytes 1048576 | tf_op jit(solution)/shard_map/jvp(jit(cumsum))/reduce_window_sum | solution.py:34
  83.9 5.1 %all-to-all-start.2 = ((bf16[128,4,512]{2,0,1:T(8,128)(2,1)}), bf16[128,4,512]{2,0,1:T(8,128)(2,1)}, u32[]{:S(2)}, u32[]{:S(2)}) async-start(bf16[128,4,512]{2,0,1:T(8,128)(2,1)} %bitcast.144), calls=%async_computation.2 | async-start | bytes 1048576 | tf_op jit(solution)/shard_map/all_to_all | solution.py:73
  95.1 2.0 reshape.161
  97.0 1.9 copy.205
  99.4 2.0 reshape.159
  103.7 2.9 %convolution_bitcast_fusion = f32[8,4,64,128]{3,0,2,1:T(8,128)S(1)} fusion(f32[4,64,128,8]{2,1,3,0:T(8,128)S(1)} %convolution_bitcast_fusion.3, f32[4,8,64]{1,2,0:T(8,128)S(1)} %copy-done.23, f32[4,8,64]{1,2,0:T(8,128)S(1)} %copy-done.24, pred[8,8]{1,0:T(8,128)(4,1)S(1)} %copy-done.32), kind=kOutput, calls=%fused_computation.4 | convolution fusion | flops 25214976 | bytes 2113600 | tf_op jit(solution)/shard_map/transpose(jvp(hnmk,mhkv->nhkv))/dot_general | solution.py:23
  106.6 2.8 %fusion.18 = (f32[4,8,64]{2,1,0:T(8,128)}, f32[4,8,64,64]{2,3,1,0:T(8,128)S(1)}, f32[4,8,64,64]{2,3,1,0:T(8,128)}) fusion(f32[4,8,64,64]{2,3,1,0:T(8,128)S(1)} %copy.195, f32[4,8,64,64]{2,1,3,0:T(8,128)S(1)} %reshape.166, f32[4,8,64]{2,1,0:T(8,128)S(1)} %slice_bitcast_fusion, bf16[4,8,64,128]{3,2,1,0:T(8,128)(2,1)S(1)} %bitcast.150, ...), kind=kOutput, calls=%fused_computation.40 | convolution fusion | flops 201979904 | bytes 3686400 | tf_op jit(solution)/shard_map/transpose(jvp(hnjk,hnjv->nhkv))/dot_general | solution.py:46
  110.4 2.5 convolution_bitcast_fusion.1
  112.9 4.3 %fusion.45 = (f32[4,8,64]{1,2,0:T(8,128)}, f32[4,8,64]{1,2,0:T(8,128)}) fusion(f32[4,8,64]{1,2,0:T(8,128)S(1)} %copy-done.23, f32[4,8,64]{1,2,0:T(8,128)S(1)} %copy-done.24, f32[8,4,64,128]{3,2,1,0:T(8,128)S(1)} %fusion.6, f32[4,64,128,8]{2,1,3,0:T(8,128)S(1)} %convolution_bitcast_fusion.3, pred[8,8]{1,0:T(8,128)(4,1)S(1)} %copy-done.32), kind=kOutput, calls=%fused_computation.83 | convolution fusion | flops 25276416 | bytes 2129984 | tf_op jit(solution)/shard_map/transpose(jvp(hnmk,mhkv->nhkv))/dot_general | solution.py:23
  117.3 2.0 convolution_bitcast_fusion.4
  122.2 1.4 copy.244
  123.6 1.4 copy.245
  125.1 1.6 convolution_select_fusion
  128.6 1.5 fusion.3
  130.1 3.7 %pad_add_fusion = (f32[4,8,64,64]{2,3,1,0:T(8,128)}, bf16[4,8,64,64]{2,3,1,0:T(8,128)(2,1)}, bf16[4,8,64,64]{2,3,1,0:T(8,128)(2,1)S(1)}) fusion(f32[4,8,1,64]{2,3,1,0:T(8,128)S(1)} %fusion.3, f32[4,8,64,64]{2,3,1,0:T(8,128)S(1)} %fusion.44, f32[4,8,64,64]{2,1,3,0:T(8,128)S(1)} %mul.72, f32[4,8,64,64]{2,3,1,0:T(8,128)S(1)} %copy.195, ...), kind=kOutput, calls=%fused_computation.22 | convolution fusion | flops 103677952 | bytes 4734976 | tf_op jit(solution)/shard_map/transpose(jvp(hnik,hnjk->hnij))/dot_general | solution.py:41
  137.1 1.7 copy.213
  138.8 4.8 %all-to-all-start.4 = ((bf16[4,128,256]{1,2,0:T(8,128)(2,1)}), bf16[4,128,256]{1,2,0:T(8,128)(2,1)S(1)}, u32[]{:S(2)}, u32[]{:S(2)}) async-start(bf16[4,128,256]{1,2,0:T(8,128)(2,1)} %copy.213), calls=%async_computation.4 | async-start | bytes 524288 | tf_op jit(solution)/shard_map/all_to_all | solution.py:101
  143.6 3.1 %convolution_select_fusion.2 = f32[4,8,64,64]{3,2,1,0:T(8,128)} fusion(pred[64,64]{1,0:T(8,128)(4,1)S(1)} %copy-done.28, f32[4,8,64,64]{2,1,3,0:T(8,128)S(1)} %reshape.166, f32[4,8,64,64]{2,3,1,0:T(8,128)S(1)} %copy.195, f32[4,8,64,64]{2,1,3,0:T(8,128)S(1)} %mul.72), kind=kOutput, calls=%fused_computation.11 | convolution fusion | flops 101187584 | bytes 2101248 | tf_op jit(solution)/shard_map/jvp(hnik,hnjk->hnij)/dot_general | solution.py:41
  148.3 3.2 %fusion.11 = f32[4,8,64,128]{3,2,1,0:T(8,128)S(1)} fusion(f32[4,8,64,64]{2,3,1,0:T(8,128)S(1)} %copy-done.4, f32[8,4,64,128]{3,0,2,1:T(8,128)} %copy-done.9), kind=kOutput, calls=%fused_computation.30 | convolution fusion | flops 201326592 | bytes 2621440 | tf_op jit(solution)/shard_map/transpose(jvp(hnjk,hnjv->nhkv))/dot_general | solution.py:46
  151.5 5.2 %all-to-all-start.6 = ((bf16[4,128,256]{1,2,0:T(8,128)(2,1)}), bf16[4,128,256]{1,2,0:T(8,128)(2,1)S(1)}, u32[]{:S(2)}, u32[]{:S(2)}) async-start(bf16[4,128,256]{1,2,0:T(8,128)(2,1)} %copy.226), calls=%async_computation.6 | async-start | bytes 524288 | tf_op jit(solution)/shard_map/all_to_all | solution.py:104
  159.6 25.8 %fusion.47 = f32[4,8,64,64]{3,1,2,0:T(8,128)S(1)} fusion(f32[4,8,64,64]{3,1,2,0:T(8,128)S(1)} %copy.246), kind=kOutput, calls=%fused_computation.85 | output fusion | flops 8257536 | bytes 1048576 | tf_op jit(solution)/shard_map/transpose(jvp(jit(cumsum)))/reduce_window_sum | solution.py:34
  186.1 5.2 %all-to-all-start.7 = ((bf16[4,128,512]{2,1,0:T(8,128)(2,1)}), bf16[4,128,512]{2,1,0:T(8,128)(2,1)S(1)}, u32[]{:S(2)}, u32[]{:S(2)}) async-start(bf16[4,128,512]{2,1,0:T(8,128)(2,1)} %convert_element_type.84), calls=%async_computation.7 | async-start | bytes 1048576 | tf_op jit(solution)/shard_map/all_to_all | solution.py:107
  193.9 56.5 %all-reduce.3.cloned.1.call-done = f32[64,256]{1,0:T(8,128)} async-done(((f32[64,256]{1,0:T(8,128)}), f32[64,256]{1,0:T(8,128)}) %all-reduce.3.cloned.1.call-update) | async-done | bytes 65552 | tf_op jit(solution)/shard_map/psum | solution.py:122
  250.4 14.1 %all_gather.7 = f32[64,1024]{1,0:T(8,128)S(1)} all-gather(f32[64,256]{1,0:T(8,128)} %all-reduce.3.cloned.1.call-done), channel_id=1, replica_groups=mesh['sp'=4,'dp'=8] {'sp'}, dimensions={1}, use_global_device_ids=true | all-gather | bytes 327680 | tf_op jit(solution)/shard_map/all_gather | solution.py:123
  (132 shorter events, 37.8 us)
Async XLA Ops:
  8.0 41.7 %copy-start = (bf16[64,1024]{1,0:T(8,128)(2,1)S(1)}, bf16[64,1024]{1,0:T(8,128)(2,1)}, u32[]{:S(2)}) copy-start(bf16[64,1024]{1,0:T(8,128)(2,1)} %param.13) | copy-start | bytes 393220
  8.0 12.1 %all-to-all-start.1 = ((bf16[128,4,4]{0,2,1:T(4,128)(2,1)}), bf16[128,4,4]{0,2,1:T(4,128)(2,1)S(1)}, u32[]{:S(2)}, u32[]{:S(2)}) async-start(bf16[128,4,4]{0,2,1:T(4,128)(2,1)} %bitcast.169), calls=%async_computation.1 | async-start | bytes 8192 | tf_op jit(solution)/shard_map/all_to_all | solution.py:75
  20.1 3.6 %copy-start.20 = (bf16[128,1024]{1,0:T(8,128)(2,1)S(1)}, bf16[128,1024]{1,0:T(8,128)(2,1)}, u32[]{:S(2)}) copy-start(bf16[128,1024]{1,0:T(8,128)(2,1)} %param.9) | copy-start | bytes 786436
  20.1 11.4 %all-to-all-start.5 = ((bf16[128,4,256]{0,2,1:T(8,128)(2,1)}), bf16[128,4,256]{0,2,1:T(8,128)(2,1)S(1)}, u32[]{:S(2)}, u32[]{:S(2)}) async-start(bf16[128,4,256]{0,2,1:T(8,128)(2,1)} %bitcast.24), calls=%async_computation.5 | async-start | bytes 524288 | tf_op jit(solution)/shard_map/all_to_all | solution.py:71
  23.6 11.3 %copy-start.17 = (bf16[128,2048]{1,0:T(8,128)(2,1)S(1)}, bf16[128,2048]{1,0:T(8,128)(2,1)}, u32[]{:S(2)}) copy-start(bf16[128,2048]{1,0:T(8,128)(2,1)} %param.11) | copy-start | bytes 1572868
  31.5 19.5 %all-to-all-start = ((bf16[128,4,256]{0,2,1:T(8,128)(2,1)}), bf16[128,4,256]{0,2,1:T(8,128)(2,1)S(1)}, u32[]{:S(2)}, u32[]{:S(2)}) async-start(bf16[128,4,256]{0,2,1:T(8,128)(2,1)} %bitcast), calls=%async_computation | async-start | bytes 524288 | tf_op jit(solution)/shard_map/all_to_all | solution.py:72
  35.0 1.6 copy-start.31
  49.0 1.9 copy-start.21
  51.0 5.4 %copy-start.18 = (bf16[128,2048]{1,0:T(8,128)(2,1)S(1)}, bf16[128,2048]{1,0:T(8,128)(2,1)}, u32[]{:S(2)}) copy-start(bf16[128,2048]{1,0:T(8,128)(2,1)} %param.10) | copy-start | bytes 1572868
  51.7 32.2 %all-to-all-start.3 = ((bf16[128,4,512]{2,0,1:T(8,128)(2,1)}), bf16[128,4,512]{2,0,1:T(8,128)(2,1)}, u32[]{:S(2)}, u32[]{:S(2)}) async-start(bf16[128,4,512]{2,0,1:T(8,128)(2,1)} %bitcast.143), calls=%async_computation.3 | async-start | bytes 1048576 | tf_op jit(solution)/shard_map/all_to_all | solution.py:74
  83.9 15.5 %all-to-all-start.2 = ((bf16[128,4,512]{2,0,1:T(8,128)(2,1)}), bf16[128,4,512]{2,0,1:T(8,128)(2,1)}, u32[]{:S(2)}, u32[]{:S(2)}) async-start(bf16[128,4,512]{2,0,1:T(8,128)(2,1)} %bitcast.144), calls=%async_computation.2 | async-start | bytes 1048576 | tf_op jit(solution)/shard_map/all_to_all | solution.py:73
  102.5 7.0 %copy-start.5 = (bf16[4,512,128]{2,1,0:T(8,128)(2,1)}, bf16[4,512,128]{2,1,0:T(8,128)(2,1)S(1)}, u32[]{:S(2)}) copy-start(bf16[4,512,128]{2,1,0:T(8,128)(2,1)S(1)} %copy.198) | copy-start | bytes 1572868
  106.6 2.9 %copy-start.9 = (f32[8,4,64,128]{3,0,2,1:T(8,128)}, f32[8,4,64,128]{3,0,2,1:T(8,128)S(1)}, u32[]{:S(2)}) copy-start(f32[8,4,64,128]{3,0,2,1:T(8,128)S(1)} %convolution_bitcast_fusion) | copy-start | bytes 3145732
  117.3 2.0 copy-start.26
  122.2 1.4 copy-start.29
  123.6 1.4 copy-start.27
  126.7 1.3 copy-start.11
  126.7 1.5 copy-start.12
  126.7 1.8 copy-start.13
  128.5 1.5 copy-start.8
  128.5 1.5 copy-start.10
  138.8 4.8 %copy-start.28 = (pred[64,64]{1,0:T(8,128)(4,1)S(1)}, pred[64,64]{1,0:T(8,128)(4,1)}, u32[]{:S(2)}) copy-start(pred[64,64]{1,0:T(8,128)(4,1)} %iota_compare_fusion) | copy-start | bytes 12292
  138.8 12.7 %all-to-all-start.4 = ((bf16[4,128,256]{1,2,0:T(8,128)(2,1)}), bf16[4,128,256]{1,2,0:T(8,128)(2,1)S(1)}, u32[]{:S(2)}, u32[]{:S(2)}) async-start(bf16[4,128,256]{1,2,0:T(8,128)(2,1)} %copy.213), calls=%async_computation.4 | async-start | bytes 524288 | tf_op jit(solution)/shard_map/all_to_all | solution.py:101
  143.6 3.1 %copy-start.14 = (bf16[4,8,64,64]{2,3,1,0:T(8,128)(2,1)S(1)}, bf16[4,8,64,64]{2,3,1,0:T(8,128)(2,1)}, u32[]{:S(2)}) copy-start(bf16[4,8,64,64]{2,3,1,0:T(8,128)(2,1)} %get-tuple-element.23) | copy-start | bytes 786436
  148.3 8.4 %copy-start.6 = (f32[4,8,64,64]{3,2,1,0:T(8,128)S(1)}, f32[4,8,64,64]{3,2,1,0:T(8,128)}, u32[]{:S(2)}) copy-start(f32[4,8,64,64]{3,2,1,0:T(8,128)} %convolution_select_fusion.2) | copy-start | bytes 1572868
  151.5 5.3 %copy-start.2 = (bf16[4,512,128]{2,1,0:T(8,128)(2,1)S(1)}, bf16[4,512,128]{2,1,0:T(8,128)(2,1)}, u32[]{:S(2)}) copy-start(bf16[4,512,128]{2,1,0:T(8,128)(2,1)} %copy.205) | copy-start | bytes 1572868
  151.5 34.6 %all-to-all-start.6 = ((bf16[4,128,256]{1,2,0:T(8,128)(2,1)}), bf16[4,128,256]{1,2,0:T(8,128)(2,1)S(1)}, u32[]{:S(2)}, u32[]{:S(2)}) async-start(bf16[4,128,256]{1,2,0:T(8,128)(2,1)} %copy.226), calls=%async_computation.6 | async-start | bytes 524288 | tf_op jit(solution)/shard_map/all_to_all | solution.py:104
  157.7 1.4 copy-start.7
  186.1 5.3 %copy-start.19 = (f32[256,512]{1,0:T(8,128)S(1)}, f32[256,512]{1,0:T(8,128)}, u32[]{:S(2)}) copy-start(f32[256,512]{1,0:T(8,128)} %get-tuple-element.30) | copy-start | bytes 1572868
  186.1 81.5 %all-to-all-start.7 = ((bf16[4,128,512]{2,1,0:T(8,128)(2,1)}), bf16[4,128,512]{2,1,0:T(8,128)(2,1)S(1)}, u32[]{:S(2)}, u32[]{:S(2)}) async-start(bf16[4,128,512]{2,1,0:T(8,128)(2,1)} %convert_element_type.84), calls=%async_computation.7 | async-start | bytes 1048576 | tf_op jit(solution)/shard_map/all_to_all | solution.py:107
  191.3 59.1 %all-reduce.3.cloned.1.call-start = ((), (), s32[]{:S(2)}) async-start(), calls=%async_computation.10 | async-start | bytes 131072 | tf_op jit(solution)/shard_map/psum | solution.py:122
  193.0 71.5 %reduce-scatter.2.cloned.1.call-start = ((), (), s32[]{:S(2)}) async-start(), calls=%async_computation.9 | async-start | bytes 163840 | tf_op jit(solution)/shard_map/reduce_scatter | solution.py:116
  (11 other events, 10.9 us)
Sparse Core Ops, SparseCore 0:
  195.7 54.6 all-reduce.2
Sparse Core Ops, SparseCore 1:
  196.3 20.9 reduce-scatter.1
where the time goes:
time: 279 us; the launch traced here: 277 us
  waiting for transfers between devices  67.7 us (24%)
  other arithmetic  56 us (20%)
  local copies, waits for them, and re-layouts  39.8 us (14%)
  starting transfers between devices  38 us (14%)
  matrix products  32.9 us (12%)
  blocking collectives  26.6 us (10%)
  between operations  15.9 us (6%)
    psum x1, waiting for transfers between devices, on_device(): summed = lax.psum(local_weight, 'dp')  56.5 us
    another operation x2, other arithmetic, gla_forward(): cumulative = jnp.cumsum(blocked(logarithm_decay), axis=2)  51.6 us
    all_gather x1, blocking collectives, on_device(): weight_grad = lax.all_gather(summed, 'sp', axis=1, tiled=True)  14.1 us
    all_gather x1, blocking collectives, on_device(): hidden_code_rows = lax.all_gather(compact_factor, 'sp', axis=0, tiled=True)  12.5 us
    unnamed x72, local copies, waits for them, and re-layouts  10.3 us
    dot_general x3, matrix products, carry_states(): return jnp.einsum('hnmk,mhkv->nhkv', weights, increments, precision=highest)  9.75 us
    dot_general x3, matrix products, gla_forward(): jnp.einsum('hnik,hnjk->hnij', query_decayed, key_inverse, precision=highest)  8.12 us
    all_to_all x1, waiting for transfers between devices, on_device(): lax.all_to_all(probe_vectors, 'sp', split_axis=1, concat_axis=0, tiled=True)  7.02 us
  transfers between devices with their start and end apart: 10, of which 4 were waited for; matrix products, arithmetic and copies ran while one was open for 31% of the time, Pallas kernels for 0%

commit v1 on v0

--- a/solution.py
+++ b/solution.py
@@ -119,7 +119,7 @@
     local_weight = jnp.einsum(
         "sr,sc->rc", hidden_code_rows, gate_grad, preferred_element_type=jnp.float32
     )
-    summed = lax.psum(local_weight, "dp")
+    summed = jnp.sum(lax.all_gather(local_weight, "dp"), axis=0)
     weight_grad = lax.all_gather(summed, "sp", axis=1, tiled=True)
     return (query_grad, key_grad, value_grad, latent_grad, weight_grad)
 

time: 279 us -> 231 us (0.83)
  waiting for transfers between devices: 67.7 us -> 11.2 us
  blocking collectives: 26.6 us -> 37 us
    psum x1 -> x0, waiting for transfers between devices: 56.5 us -> none  [on_device(): summed = lax.psum(local_weight, 'dp')]
    all_gather x0 -> x1, blocking collectives: none -> 9.86 us  [on_device(): summed = jnp.sum(lax.all_gather(local_weight, 'dp'), axis=0)]
  transfers between devices with their start and end apart: 10 -> 9, of which waited for: 4 -> 3; matrix products, arithmetic and copies ran while one was open for 31% -> 37% of each run, Pallas kernels for 0% -> 0%
where the time goes in v1:
time: 231 us; the launch traced here: 229 us
  other arithmetic  56 us (24%)
  local copies, waits for them, and re-layouts  40 us (17%)
  starting transfers between devices  38 us (16%)
  blocking collectives  37 us (16%)
  matrix products  32.3 us (14%)
  between operations  14.5 us (6%)
  waiting for transfers between devices  11.2 us (5%)
    another operation x2, other arithmetic, gla_forward(): cumulative = jnp.cumsum(blocked(logarithm_decay), axis=2)  51.6 us
    all_gather x1, blocking collectives, on_device(): weight_grad = lax.all_gather(summed, 'sp', axis=1, tiled=True)  14.7 us
    all_gather x1, blocking collectives, on_device(): hidden_code_rows = lax.all_gather(compact_factor, 'sp', axis=0, tiled=True)  12.5 us
    unnamed x72, local copies, waits for them, and re-layouts  10.4 us
    all_gather x1, blocking collectives, on_device(): summed = jnp.sum(lax.all_gather(local_weight, 'dp'), axis=0)  9.86 us
    dot_general x3, matrix products, carry_states(): return jnp.einsum('hnmk,mhkv->nhkv', weights, increments, precision=highest)  9.76 us
    dot_general x3, matrix products, gla_forward(): jnp.einsum('hnik,hnjk->hnij', query_decayed, key_inverse, precision=highest)  8.14 us
    all_to_all x1, waiting for transfers between devices, on_device(): lax.all_to_all(probe_vectors, 'sp', split_axis=1, concat_axis=0, tiled=True)  7.02 us
  transfers between devices with their start and end apart: 9, of which 3 were waited for; matrix products, arithmetic and copies ran while one was open for 37% of the time, Pallas kernels for 0%

profile of v1, /device:TPU:0, one launch (start us, length us, event | category | flops | bytes accessed | tf_op | source)
XLA Modules:
  0.0 229.0 jit_solution(18394739539287099076)
XLA Ops:
  7.2 6.5 %all-to-all-start.1 = ((bf16[128,4,4]{0,2,1:T(4,128)(2,1)}), bf16[128,4,4]{0,2,1:T(4,128)(2,1)S(1)}, u32[]{:S(2)}, u32[]{:S(2)}) async-start(bf16[128,4,4]{0,2,1:T(4,128)(2,1)} %bitcast.171), calls=%async_computation.1 | async-start | bytes 8192 | tf_op jit(solution)/shard_map/all_to_all | solution.py:75
  13.7 1.8 copy.214
  15.5 3.8 %all-to-all-done.1 = bf16[128,4,4]{0,2,1:T(4,128)(2,1)S(1)} async-done(((bf16[128,4,4]{0,2,1:T(4,128)(2,1)}), bf16[128,4,4]{0,2,1:T(4,128)(2,1)S(1)}, u32[]{:S(2)}, u32[]{:S(2)}) %all-to-all-start.1) | async-done | bytes 4128 | tf_op jit(solution)/shard_map/all_to_all | solution.py:75
  19.3 3.5 %all-to-all-start.5 = ((bf16[128,4,256]{0,2,1:T(8,128)(2,1)}), bf16[128,4,256]{0,2,1:T(8,128)(2,1)S(1)}, u32[]{:S(2)}, u32[]{:S(2)}) async-start(bf16[128,4,256]{0,2,1:T(8,128)(2,1)} %bitcast.24), calls=%async_computation.5 | async-start | bytes 524288 | tf_op jit(solution)/shard_map/all_to_all | solution.py:71
  23.7 7.0 %all-to-all-done.5 = bf16[128,4,256]{0,2,1:T(8,128)(2,1)S(1)} async-done(((bf16[128,4,256]{0,2,1:T(8,128)(2,1)}), bf16[128,4,256]{0,2,1:T(8,128)(2,1)S(1)}, u32[]{:S(2)}, u32[]{:S(2)}) %all-to-all-start.5) | async-done | bytes 262176 | tf_op jit(solution)/shard_map/all_to_all | solution.py:71
  30.7 3.4 %all-to-all-start = ((bf16[128,4,256]{0,2,1:T(8,128)(2,1)}), bf16[128,4,256]{0,2,1:T(8,128)(2,1)S(1)}, u32[]{:S(2)}, u32[]{:S(2)}) async-start(bf16[128,4,256]{0,2,1:T(8,128)(2,1)} %bitcast), calls=%async_computation | async-start | bytes 524288 | tf_op jit(solution)/shard_map/all_to_all | solution.py:72
  35.8 12.5 %all_gather.12 = bf16[512,64]{0,1:T(8,128)(2,1)S(1)} all-gather(bf16[128,64]{0,1:T(8,128)(2,1)S(1)} %copy-done.31), channel_id=1, replica_groups=mesh['sp'=4,'dp'=8] {'sp'}, dimensions={0}, use_global_device_ids=true | all-gather | bytes 81920 | tf_op jit(solution)/shard_map/all_gather | solution.py:78
  50.9 4.1 %all-to-all-start.3 = ((bf16[128,4,512]{2,0,1:T(8,128)(2,1)}), bf16[128,4,512]{2,0,1:T(8,128)(2,1)}, u32[]{:S(2)}, u32[]{:S(2)}) async-start(bf16[128,4,512]{2,0,1:T(8,128)(2,1)} %bitcast.144), calls=%async_computation.3 | async-start | bytes 1048576 | tf_op jit(solution)/shard_map/all_to_all | solution.py:74
  57.2 25.9 %fusion.46 = f32[4,8,64,64]{3,1,2,0:T(8,128)S(1)} fusion(f32[4,8,64,64]{3,1,2,0:T(8,128)S(1)} %copy.194), kind=kOutput, calls=%fused_computation.84 | output fusion | flops 8257536 | bytes 1048576 | tf_op jit(solution)/shard_map/jvp(jit(cumsum))/reduce_window_sum | solution.py:34
  83.1 5.1 %all-to-all-start.2 = ((bf16[128,4,512]{2,0,1:T(8,128)(2,1)}), bf16[128,4,512]{2,0,1:T(8,128)(2,1)}, u32[]{:S(2)}, u32[]{:S(2)}) async-start(bf16[128,4,512]{2,0,1:T(8,128)(2,1)} %bitcast.145), calls=%async_computation.2 | async-start | bytes 1048576 | tf_op jit(solution)/shard_map/all_to_all | solution.py:73
  94.3 2.0 reshape.161
  96.2 1.9 copy.205
  98.5 2.0 reshape.159
  102.9 2.9 %convolution_bitcast_fusion = f32[8,4,64,128]{3,0,2,1:T(8,128)S(1)} fusion(f32[4,64,128,8]{2,1,3,0:T(8,128)S(1)} %convolution_bitcast_fusion.3, f32[4,8,64]{1,2,0:T(8,128)S(1)} %copy-done.23, f32[4,8,64]{1,2,0:T(8,128)S(1)} %copy-done.24, pred[8,8]{1,0:T(8,128)(4,1)S(1)} %copy-done.32), kind=kOutput, calls=%fused_computation.4 | convolution fusion | flops 25214976 | bytes 2113600 | tf_op jit(solution)/shard_map/transpose(jvp(hnmk,mhkv->nhkv))/dot_general | solution.py:23
  105.8 2.8 %fusion.18 = (f32[4,8,64]{2,1,0:T(8,128)}, f32[4,8,64,64]{2,3,1,0:T(8,128)S(1)}, f32[4,8,64,64]{2,3,1,0:T(8,128)}) fusion(f32[4,8,64,64]{2,3,1,0:T(8,128)S(1)} %copy.195, f32[4,8,64,64]{2,1,3,0:T(8,128)S(1)} %reshape.166, f32[4,8,64]{2,1,0:T(8,128)S(1)} %slice_bitcast_fusion, bf16[4,8,64,128]{3,2,1,0:T(8,128)(2,1)S(1)} %bitcast.151, ...), kind=kOutput, calls=%fused_computation.40 | convolution fusion | flops 201979904 | bytes 3686400 | tf_op jit(solution)/shard_map/transpose(jvp(hnjk,hnjv->nhkv))/dot_general | solution.py:46
  109.6 2.5 %convolution_bitcast_fusion.1 = f32[8,4,64,128]{3,0,2,1:T(8,128)S(1)} fusion(f32[8,4,64,128]{3,2,1,0:T(8,128)S(1)} %fusion.6, f32[4,8,64]{1,2,0:T(8,128)S(1)} %copy-done.23, f32[4,8,64]{1,2,0:T(8,128)S(1)} %copy-done.24, pred[8,8]{1,0:T(8,128)(4,1)S(1)} %copy-done.32), kind=kOutput, calls=%fused_computation.6 | convolution fusion | flops 25214976 | bytes 2113600 | tf_op jit(solution)/shard_map/jvp(hnmk,mhkv->nhkv)/dot_general | solution.py:23
  112.1 4.3 %fusion.45 = (f32[4,8,64]{1,2,0:T(8,128)}, f32[4,8,64]{1,2,0:T(8,128)}) fusion(f32[4,8,64]{1,2,0:T(8,128)S(1)} %copy-done.23, f32[4,8,64]{1,2,0:T(8,128)S(1)} %copy-done.24, f32[8,4,64,128]{3,2,1,0:T(8,128)S(1)} %fusion.6, f32[4,64,128,8]{2,1,3,0:T(8,128)S(1)} %convolution_bitcast_fusion.3, pred[8,8]{1,0:T(8,128)(4,1)S(1)} %copy-done.32), kind=kOutput, calls=%fused_computation.83 | convolution fusion | flops 25276416 | bytes 2129984 | tf_op jit(solution)/shard_map/transpose(jvp(hnmk,mhkv->nhkv))/dot_general | solution.py:23
  116.4 2.0 convolution_bitcast_fusion.4
  121.4 1.4 copy.244
  122.8 1.4 copy.245
  124.2 1.6 convolution_select_fusion
  127.7 1.5 fusion.3
  129.2 3.7 %pad_add_fusion = (f32[4,8,64,64]{2,3,1,0:T(8,128)}, bf16[4,8,64,64]{2,3,1,0:T(8,128)(2,1)}, bf16[4,8,64,64]{2,3,1,0:T(8,128)(2,1)S(1)}) fusion(f32[4,8,1,64]{2,3,1,0:T(8,128)S(1)} %fusion.3, f32[4,8,64,64]{2,3,1,0:T(8,128)S(1)} %fusion.44, f32[4,8,64,64]{2,1,3,0:T(8,128)S(1)} %mul.72, f32[4,8,64,64]{2,3,1,0:T(8,128)S(1)} %copy.195, ...), kind=kOutput, calls=%fused_computation.22 | convolution fusion | flops 103677952 | bytes 4734976 | tf_op jit(solution)/shard_map/transpose(jvp(hnik,hnjk->hnij))/dot_general | solution.py:41
  136.3 1.7 copy.213
  137.9 4.8 %all-to-all-start.4 = ((bf16[4,128,256]{1,2,0:T(8,128)(2,1)}), bf16[4,128,256]{1,2,0:T(8,128)(2,1)S(1)}, u32[]{:S(2)}, u32[]{:S(2)}) async-start(bf16[4,128,256]{1,2,0:T(8,128)(2,1)} %copy.213), calls=%async_computation.4 | async-start | bytes 524288 | tf_op jit(solution)/shard_map/all_to_all | solution.py:101
  142.8 3.1 %convolution_select_fusion.2 = f32[4,8,64,64]{3,2,1,0:T(8,128)} fusion(pred[64,64]{1,0:T(8,128)(4,1)S(1)} %copy-done.28, f32[4,8,64,64]{2,1,3,0:T(8,128)S(1)} %reshape.166, f32[4,8,64,64]{2,3,1,0:T(8,128)S(1)} %copy.195, f32[4,8,64,64]{2,1,3,0:T(8,128)S(1)} %mul.72), kind=kOutput, calls=%fused_computation.11 | convolution fusion | flops 101187584 | bytes 2101248 | tf_op jit(solution)/shard_map/jvp(hnik,hnjk->hnij)/dot_general | solution.py:41
  147.5 3.2 %fusion.11 = f32[4,8,64,128]{3,2,1,0:T(8,128)S(1)} fusion(f32[4,8,64,64]{2,3,1,0:T(8,128)S(1)} %copy-done.4, f32[8,4,64,128]{3,0,2,1:T(8,128)} %copy-done.9), kind=kOutput, calls=%fused_computation.30 | convolution fusion | flops 201326592 | bytes 2621440 | tf_op jit(solution)/shard_map/transpose(jvp(hnjk,hnjv->nhkv))/dot_general | solution.py:46
  150.7 5.2 %all-to-all-start.6 = ((bf16[4,128,256]{1,2,0:T(8,128)(2,1)}), bf16[4,128,256]{1,2,0:T(8,128)(2,1)S(1)}, u32[]{:S(2)}, u32[]{:S(2)}) async-start(bf16[4,128,256]{1,2,0:T(8,128)(2,1)} %copy.226), calls=%async_computation.6 | async-start | bytes 524288 | tf_op jit(solution)/shard_map/all_to_all | solution.py:104
  158.8 25.8 %fusion.47 = f32[4,8,64,64]{3,1,2,0:T(8,128)S(1)} fusion(f32[4,8,64,64]{3,1,2,0:T(8,128)S(1)} %copy.246), kind=kOutput, calls=%fused_computation.85 | output fusion | flops 8257536 | bytes 1048576 | tf_op jit(solution)/shard_map/transpose(jvp(jit(cumsum)))/reduce_window_sum | solution.py:34
  185.3 5.2 %all-to-all-start.7 = ((bf16[4,128,512]{2,1,0:T(8,128)(2,1)}), bf16[4,128,512]{2,1,0:T(8,128)(2,1)S(1)}, u32[]{:S(2)}, u32[]{:S(2)}) async-start(bf16[4,128,512]{2,1,0:T(8,128)(2,1)} %convert_element_type.84), calls=%async_computation.7 | async-start | bytes 1048576 | tf_op jit(solution)/shard_map/all_to_all | solution.py:107
  192.6 9.9 %all-gather = f32[512,256]{1,0:T(8,128)S(1)} all-gather(f32[64,256]{1,0:T(8,128)S(1)} %convolution_bitcast_fusion.5), channel_id=2, replica_groups=mesh['sp'=4,'dp'=8] {'dp'}, dimensions={0}, use_global_device_ids=true | all-gather | bytes 589824 | tf_op jit(solution)/shard_map/all_gather | solution.py:122
  202.4 14.7 %all_gather.15 = f32[64,1024]{1,0:T(8,128)S(1)} all-gather(f32[64,256]{1,0:T(8,128)S(1)} %reduce_sum.50), channel_id=1, replica_groups=mesh['sp'=4,'dp'=8] {'sp'}, dimensions={1}, use_global_device_ids=true | all-gather | bytes 327680 | tf_op jit(solution)/shard_map/all_gather | solution.py:123
  (131 shorter events, 37.3 us)
Async XLA Ops:
  7.2 41.7 %copy-start = (bf16[64,1024]{1,0:T(8,128)(2,1)S(1)}, bf16[64,1024]{1,0:T(8,128)(2,1)}, u32[]{:S(2)}) copy-start(bf16[64,1024]{1,0:T(8,128)(2,1)} %param.13) | copy-start | bytes 393220
  7.2 12.1 %all-to-all-start.1 = ((bf16[128,4,4]{0,2,1:T(4,128)(2,1)}), bf16[128,4,4]{0,2,1:T(4,128)(2,1)S(1)}, u32[]{:S(2)}, u32[]{:S(2)}) async-start(bf16[128,4,4]{0,2,1:T(4,128)(2,1)} %bitcast.171), calls=%async_computation.1 | async-start | bytes 8192 | tf_op jit(solution)/shard_map/all_to_all | solution.py:75
  19.3 3.6 %copy-start.20 = (bf16[128,1024]{1,0:T(8,128)(2,1)S(1)}, bf16[128,1024]{1,0:T(8,128)(2,1)}, u32[]{:S(2)}) copy-start(bf16[128,1024]{1,0:T(8,128)(2,1)} %param.9) | copy-start | bytes 786436
  19.3 11.4 %all-to-all-start.5 = ((bf16[128,4,256]{0,2,1:T(8,128)(2,1)}), bf16[128,4,256]{0,2,1:T(8,128)(2,1)S(1)}, u32[]{:S(2)}, u32[]{:S(2)}) async-start(bf16[128,4,256]{0,2,1:T(8,128)(2,1)} %bitcast.24), calls=%async_computation.5 | async-start | bytes 524288 | tf_op jit(solution)/shard_map/all_to_all | solution.py:71
  22.8 11.3 %copy-start.17 = (bf16[128,2048]{1,0:T(8,128)(2,1)S(1)}, bf16[128,2048]{1,0:T(8,128)(2,1)}, u32[]{:S(2)}) copy-start(bf16[128,2048]{1,0:T(8,128)(2,1)} %param.11) | copy-start | bytes 1572868
  30.7 19.5 %all-to-all-start = ((bf16[128,4,256]{0,2,1:T(8,128)(2,1)}), bf16[128,4,256]{0,2,1:T(8,128)(2,1)S(1)}, u32[]{:S(2)}, u32[]{:S(2)}) async-start(bf16[128,4,256]{0,2,1:T(8,128)(2,1)} %bitcast), calls=%async_computation | async-start | bytes 524288 | tf_op jit(solution)/shard_map/all_to_all | solution.py:72
  34.1 1.6 copy-start.31
  48.3 1.9 copy-start.21
  50.2 5.4 %copy-start.18 = (bf16[128,2048]{1,0:T(8,128)(2,1)S(1)}, bf16[128,2048]{1,0:T(8,128)(2,1)}, u32[]{:S(2)}) copy-start(bf16[128,2048]{1,0:T(8,128)(2,1)} %param.10) | copy-start | bytes 1572868
  50.9 32.2 %all-to-all-start.3 = ((bf16[128,4,512]{2,0,1:T(8,128)(2,1)}), bf16[128,4,512]{2,0,1:T(8,128)(2,1)}, u32[]{:S(2)}, u32[]{:S(2)}) async-start(bf16[128,4,512]{2,0,1:T(8,128)(2,1)} %bitcast.144), calls=%async_computation.3 | async-start | bytes 1048576 | tf_op jit(solution)/shard_map/all_to_all | solution.py:74
  83.1 15.5 %all-to-all-start.2 = ((bf16[128,4,512]{2,0,1:T(8,128)(2,1)}), bf16[128,4,512]{2,0,1:T(8,128)(2,1)}, u32[]{:S(2)}, u32[]{:S(2)}) async-start(bf16[128,4,512]{2,0,1:T(8,128)(2,1)} %bitcast.145), calls=%async_computation.2 | async-start | bytes 1048576 | tf_op jit(solution)/shard_map/all_to_all | solution.py:73
  101.7 7.0 %copy-start.5 = (bf16[4,512,128]{2,1,0:T(8,128)(2,1)}, bf16[4,512,128]{2,1,0:T(8,128)(2,1)S(1)}, u32[]{:S(2)}) copy-start(bf16[4,512,128]{2,1,0:T(8,128)(2,1)S(1)} %copy.198) | copy-start | bytes 1572868
  105.8 2.9 %copy-start.9 = (f32[8,4,64,128]{3,0,2,1:T(8,128)}, f32[8,4,64,128]{3,0,2,1:T(8,128)S(1)}, u32[]{:S(2)}) copy-start(f32[8,4,64,128]{3,0,2,1:T(8,128)S(1)} %convolution_bitcast_fusion) | copy-start | bytes 3145732
  116.4 2.0 copy-start.26
  121.4 1.4 copy-start.29
  122.8 1.4 copy-start.27
  125.8 1.3 copy-start.11
  125.8 1.5 copy-start.12
  125.8 1.8 copy-start.13
  127.7 1.5 copy-start.8
  127.7 1.5 copy-start.10
  137.9 4.9 %copy-start.28 = (pred[64,64]{1,0:T(8,128)(4,1)S(1)}, pred[64,64]{1,0:T(8,128)(4,1)}, u32[]{:S(2)}) copy-start(pred[64,64]{1,0:T(8,128)(4,1)} %iota_compare_fusion) | copy-start | bytes 12292
  137.9 12.7 %all-to-all-start.4 = ((bf16[4,128,256]{1,2,0:T(8,128)(2,1)}), bf16[4,128,256]{1,2,0:T(8,128)(2,1)S(1)}, u32[]{:S(2)}, u32[]{:S(2)}) async-start(bf16[4,128,256]{1,2,0:T(8,128)(2,1)} %copy.213), calls=%async_computation.4 | async-start | bytes 524288 | tf_op jit(solution)/shard_map/all_to_all | solution.py:101
  142.8 3.1 %copy-start.14 = (bf16[4,8,64,64]{2,3,1,0:T(8,128)(2,1)S(1)}, bf16[4,8,64,64]{2,3,1,0:T(8,128)(2,1)}, u32[]{:S(2)}) copy-start(bf16[4,8,64,64]{2,3,1,0:T(8,128)(2,1)} %get-tuple-element.23) | copy-start | bytes 786436
  146.3 1.2 copy-start.4
  147.5 8.4 %copy-start.6 = (f32[4,8,64,64]{3,2,1,0:T(8,128)S(1)}, f32[4,8,64,64]{3,2,1,0:T(8,128)}, u32[]{:S(2)}) copy-start(f32[4,8,64,64]{3,2,1,0:T(8,128)} %convolution_select_fusion.2) | copy-start | bytes 1572868
  150.7 5.3 %copy-start.2 = (bf16[4,512,128]{2,1,0:T(8,128)(2,1)S(1)}, bf16[4,512,128]{2,1,0:T(8,128)(2,1)}, u32[]{:S(2)}) copy-start(bf16[4,512,128]{2,1,0:T(8,128)(2,1)} %copy.205) | copy-start | bytes 1572868
  150.7 34.6 %all-to-all-start.6 = ((bf16[4,128,256]{1,2,0:T(8,128)(2,1)}), bf16[4,128,256]{1,2,0:T(8,128)(2,1)S(1)}, u32[]{:S(2)}, u32[]{:S(2)}) async-start(bf16[4,128,256]{1,2,0:T(8,128)(2,1)} %copy.226), calls=%async_computation.6 | async-start | bytes 524288 | tf_op jit(solution)/shard_map/all_to_all | solution.py:104
  156.9 1.4 copy-start.7
  185.3 5.3 %copy-start.19 = (f32[256,512]{1,0:T(8,128)S(1)}, f32[256,512]{1,0:T(8,128)}, u32[]{:S(2)}) copy-start(f32[256,512]{1,0:T(8,128)} %get-tuple-element.30) | copy-start | bytes 1572868
  185.3 34.9 %all-to-all-start.7 = ((bf16[4,128,512]{2,1,0:T(8,128)(2,1)}), bf16[4,128,512]{2,1,0:T(8,128)(2,1)S(1)}, u32[]{:S(2)}, u32[]{:S(2)}) async-start(bf16[4,128,512]{2,1,0:T(8,128)(2,1)} %convert_element_type.84), calls=%async_computation.7 | async-start | bytes 1048576 | tf_op jit(solution)/shard_map/all_to_all | solution.py:107
  190.5 26.6 %reduce-scatter.2.cloned.1.call-start = ((), (), s32[]{:S(2)}) async-start(), calls=%async_computation.9 | async-start | bytes 163840 | tf_op jit(solution)/shard_map/reduce_scatter | solution.py:116
  (10 other events, 9.6 us)
Sparse Core Ops, SparseCore 0:
  194.1 21.3 reduce-scatter.1
